TPU v7x, 32 devices: a whole 2x2x4 slice. The times are simulated.
32 devices in a mesh: sp: 8 (over z, y), tp: 4 (over x, core).
Axes of the slice: x: 2, y: 2, z: 4, core: 2. Of those that a mesh axis runs over, the one named last changes fastest.
Arguments:
- residual: bfloat16 [4, 768, 2048], P('tp', 'sp'), may hold values from -3 to 3
- query_nope: bfloat16 [4, 768, 1024], P('tp', 'sp'), may hold values from -9 to 9
- query_rope: bfloat16 [4, 768, 512], P('tp', 'sp'), may hold values from -48 to 48
- latent: bfloat16 [4, 768, 128], P('tp', 'sp'), may hold values from -6 to 6
- rope_key: bfloat16 [4, 768, 32], P('tp', 'sp'), may hold values from -48 to 48
- latent_gain: float32 [128], replicated, may hold values from 0.1 to 1.9
- up_key: bfloat16 [128, 1024], replicated, may hold values from -1 to 1
- up_value: bfloat16 [128, 1024], replicated, may hold values from -0.5 to 0.5
- out_weight: bfloat16 [1024, 2048], replicated, may hold values from -0.375 to 0.375
- ffn_gain: float32 [2048], replicated, may hold values from 0.1 to 1.9
- routes: int32 [4, 768, 2], P(None, 'sp'), may hold values from 0 to 7, all different within a row; in each aligned block of 96 rows (0 to 95, 96 to 191, ..., all dimensions but the last counted through in order) at most 30 rows name the same one
- route_weight: float32 [4, 768, 2], P('tp', 'sp'), may hold values from 0.1 to 1
- gate_weight: bfloat16 [8, 2048, 1024], P('sp', None, 'tp'), may hold values from -1.5 to 1.5
- up_weight: bfloat16 [8, 2048, 1024], P('sp', None, 'tp'), may hold values from -1.5 to 1.5
- down_weight: bfloat16 [8, 1024, 2048], P('sp', 'tp'), may hold values from -0.046875 to 0.046875
Outputs:
- updated: bfloat16 [4, 768, 2048], P('tp', 'sp')
Inputs may be any that keep to these rules, and one draw needn't show every extreme that they name: `routes`: each row names 2 different experts. In each aligned block of 96 rows (one sequence's rows of one device) no expert is named by more than 30 rows, a bound that some block reaches.
All inputs are finite; a program needn't handle non-finite values.
Results may differ from a plain program's by a relative error of at most 0.017.
Values may be sent and summed in bfloat16 or wider, within the bound.
A program may use at most 64 MiB of HBM per device.

v0:
```python
import math

import jax
import jax.numpy as jnp
from jax import lax
from jax.sharding import PartitionSpec as P

HEADS = 16
NOPE = 64
ROPE = 32
VDIM = 64
LATENT = 128
TOPK = 2


EPS = 1e-06
ROPE_BASE = 10000.0
CLAMP = 7.0
ALPHA = 1.702
NEG_BIG = -1e30


def rotate(values, positions, width):
    half = width // 2
    inverse = ROPE_BASE ** (-jnp.arange(half, dtype=jnp.float32) * 2.0 / width)
    angle = positions.astype(jnp.float32)[:, None] * inverse[None, :]
    cosine = jnp.cos(angle)[:, None, :]
    sine = jnp.sin(angle)[:, None, :]
    first = values[..., :half]
    second = values[..., half:]
    return jnp.concatenate(
        [first * cosine - second * sine, first * sine + second * cosine], axis=-1
    )


def rms_scaled(values, gain):
    return values * lax.rsqrt(jnp.mean(values * values, axis=-1, keepdims=True) + EPS) * gain


def block_rows(rows):
    return math.gcd(rows, 512)


def expert_term(rows, gate_w, up_w, down_w):
    gate = jnp.minimum(jnp.dot(rows, gate_w, preferred_element_type=jnp.float32), CLAMP)
    lift = jnp.clip(jnp.dot(rows, up_w, preferred_element_type=jnp.float32), -CLAMP, CLAMP)
    active = (gate * jax.nn.sigmoid(ALPHA * gate) * (lift + 1.0)).astype(jnp.bfloat16)
    return jnp.dot(active, down_w, preferred_element_type=jnp.float32)


def assign(picks, slots, count):
    flat = picks.reshape(-1)
    hot = (flat[:, None] == jnp.arange(count, dtype=jnp.int32)[None, :]).astype(jnp.int32)
    ranks = jnp.sum((jnp.cumsum(hot, axis=0) - 1) * hot, axis=1)
    return flat * slots + ranks


def pack_rows(rows, target, slots, count):
    tokens = rows.shape[0]
    owner = jnp.arange(target.shape[0], dtype=jnp.int32) // (target.shape[0] // tokens)
    source = jnp.full((count * slots,), tokens, jnp.int32).at[target].set(owner)
    padded = jnp.concatenate([rows, jnp.zeros((1, rows.shape[1]), rows.dtype)], axis=0)
    return padded[source]


def local(
    residual,
    query_nope,
    query_rope,
    latent,
    rope_key,
    latent_gain,
    up_key,
    up_value,
    out_weight,
    ffn_gain,
    routes,
    route_weight,
    gate_weight,
    up_weight,
    down_weight,
):
    tokens = residual.shape[1]
    width = residual.shape[2]
    experts = lax.axis_size("sp")
    slots = min(tokens, max(2, 5 * tokens * TOPK // (4 * experts)))
    positions = lax.axis_index("sp") * tokens + jnp.arange(tokens, dtype=jnp.int32)
    factor = (NOPE + ROPE) ** (-0.5)
    normed = rms_scaled(latent[0].astype(jnp.float32), latent_gain).astype(jnp.bfloat16)
    key_turned = rotate(rope_key[0].astype(jnp.float32)[:, None, :], positions, ROPE)[
        :, 0, :
    ].astype(jnp.bfloat16)
    query_plain = query_nope[0].reshape(tokens, HEADS, NOPE)
    query_turned = rotate(
        query_rope[0].astype(jnp.float32).reshape(tokens, HEADS, ROPE), positions, ROPE
    ).astype(jnp.bfloat16)
    initial = (
        jnp.full((HEADS, tokens), NEG_BIG, jnp.float32),
        jnp.zeros((HEADS, tokens), jnp.float32),
        jnp.zeros((tokens, HEADS, VDIM), jnp.float32),
    )
    carry = initial
    piece = (
        lax.all_gather(normed, "sp", axis=0, tiled=True),
        lax.all_gather(key_turned, "sp", axis=0, tiled=True),
    )
    rows = piece[0].shape[0]
    span = block_rows(rows)
    latent_blocks = piece[0].reshape(rows // span, span, LATENT)
    turned_blocks = piece[1].reshape(rows // span, span, ROPE)

    def step(state, blocks):
        peak_old, total, summed = state
        keys = jnp.dot(blocks[0], up_key, preferred_element_type=jnp.float32).astype(jnp.bfloat16)
        keys = keys.reshape(span, HEADS, NOPE)
        values = jnp.dot(blocks[0], up_value, preferred_element_type=jnp.float32).astype(
            jnp.bfloat16
        )
        values = values.reshape(span, HEADS, VDIM)
        scores = (
            jnp.einsum("qhd,khd->hqk", query_plain, keys, preferred_element_type=jnp.float32)
            + jnp.einsum("qhd,kd->hqk", query_turned, blocks[1], preferred_element_type=jnp.float32)
        ) * factor
        peak = jnp.maximum(peak_old, jnp.max(scores, axis=-1))
        shrink = jnp.exp(peak_old - peak)
        weights = jnp.exp(scores - peak[:, :, None])
        total = total * shrink + jnp.sum(weights, axis=-1)
        mixed = jnp.einsum(
            "hqk,khd->qhd", weights.astype(jnp.bfloat16), values, preferred_element_type=jnp.float32
        )
        summed = summed * jnp.transpose(shrink)[:, :, None] + mixed
        return ((peak, total, summed), None)

    carry, _ = lax.scan(step, carry, (latent_blocks, turned_blocks))
    peak, total, summed = carry
    attended = (
        (summed / jnp.transpose(total)[:, :, None])
        .reshape(tokens, HEADS * VDIM)
        .astype(jnp.bfloat16)
    )
    projected = jnp.dot(attended, out_weight, preferred_element_type=jnp.float32)
    middle = (residual[0].astype(jnp.float32) + projected).astype(jnp.bfloat16)
    middle_wide = middle.astype(jnp.float32)
    normal_rows = rms_scaled(middle_wide, ffn_gain).astype(jnp.bfloat16)
    own_picks = lax.dynamic_index_in_dim(routes, lax.axis_index("tp"), 0, keepdims=False)
    own_target = assign(own_picks, slots, experts)
    outgoing = pack_rows(normal_rows, own_target, slots, experts).reshape(1, experts, slots, width)
    arrived = lax.all_to_all(outgoing, "sp", split_axis=1, concat_axis=1, tiled=True)
    terms = expert_term(
        lax.all_gather(arrived, "tp", axis=0, tiled=True).reshape(-1, width),
        gate_weight[0],
        up_weight[0],
        down_weight[0],
    )
    mine = lax.psum_scatter(terms.astype(jnp.bfloat16), "tp", scatter_dimension=0, tiled=True)
    returned = lax.all_to_all(
        mine.reshape(1, experts, slots, width), "sp", split_axis=1, concat_axis=1, tiled=True
    )
    picked = returned.reshape(experts * slots, width)[own_target].reshape(tokens, TOPK, width)
    combined = jnp.sum(picked.astype(jnp.float32) * route_weight[0][:, :, None], axis=1)
    return (middle_wide + combined).astype(jnp.bfloat16)[None]


def solution(mesh):
    in_specs = (
        P("tp", "sp", None),
        P("tp", "sp", None),
        P("tp", "sp", None),
        P("tp", "sp", None),
        P("tp", "sp", None),
        P(),
        P(),
        P(),
        P(),
        P(),
        P(None, "sp", None),
        P("tp", "sp", None),
        P("sp", None, "tp"),
        P("sp", None, "tp"),
        P("sp", "tp", None),
    )
    out_specs = P("tp", "sp", None)
    return jax.shard_map(local, mesh=mesh, in_specs=in_specs, out_specs=out_specs, check_vma=False)
```

profile of v0, /device:TPU:0, one launch (start us, length us, event | category | flops | bytes accessed | tf_op | source)
XLA Modules:
  0.0 285.2 jit_solution(8489566156841574619)
XLA Ops:
  9.3 32.8 %all-gather = bf16[768,1,32]{2,1,0:T(2,128)(2,1)S(1)} all-gather(bf16[96,1,32]{2,1,0:T(2,128)(2,1)S(1)} %copy.46), channel_id=2, replica_groups=mesh['sp'=8,'tp'=4] {'sp'}, dimensions={0}, use_global_device_ids=true | all-gather | bytes 55296 | tf_op jit(solution)/shard_map/all_gather | solution.py:105
  42.8 32.6 %all_gather.9 = bf16[768,128]{1,0:T(8,128)(2,1)} all-gather(bf16[96,128]{1,0:T(8,128)(2,1)S(1)} %fusion.39), channel_id=1, replica_groups=mesh['sp'=8,'tp'=4] {'sp'}, dimensions={0}, use_global_device_ids=true | all-gather | bytes 221184 | tf_op jit(solution)/shard_map/all_gather | solution.py:104
  75.5 25.8 %while.15 = (s32[]{:T(128)}, f32[16,96]{1,0:T(8,128)S(1)}, f32[16,96]{1,0:T(8,128)}, f32[96,16,64]{0,2,1:T(8,128)}, bf16[3,256,128]{2,1,0:T(8,128)(2,1)}, /*inde...) while((s32[]{:T(128)}, f32[16,96]{1,0:T(8,128)S(1)}, ...), condition=%wide.region_4.5_spmd.clone, body=%wide.region_1.4_spmd.clone.sunk | while | flops 263627776 | bytes 14435629 | solution.py:134
  75.6 1.3 convolution_convert_fusion.5
  78.1 1.3 convolution_convert_fusion.6
  80.4 2.3 fusion.97
  84.0 1.3 convolution_convert_fusion.5
  86.6 1.3 convolution_convert_fusion.6
  88.9 2.5 fusion.97
  92.7 1.3 convolution_convert_fusion.5
  95.2 1.3 convolution_convert_fusion.6
  97.5 2.5 fusion.97
  101.3 1.1 divide_convert_fusion
  102.4 3.2 %multiply_reduce_fusion.1 = (f32[96]{0:T(128)S(1)}, f32[96,2048]{1,0:T(8,128)S(1)}) fusion(bf16[96,1024]{0,1:T(8,128)(2,1)S(1)} %bitcast.107, bf16[1024,2048]{1,0:T(8,128)(2,1)} %param.25, bf16[1,96,2048]{2,1,0:T(8,128)(2,1)} %param.17), kind=kOutput, calls=%fused_computation.49 | convolution fusion | flops 403832736 | bytes 5570944 | tf_op jit(solution)/shard_map/dot_general | solution.py:141
  107.8 1.4 scatter_custom_fusion
  109.4 2.3 gather_fusion
  111.7 1.5 reshape.223
  113.1 21.4 %all_to_all.10 = bf16[1,8,30,2048]{3,2,0,1:T(8,128)(2,1)S(1)} all-to-all(bf16[1,8,30,2048]{3,2,0,1:T(8,128)(2,1)S(1)} %bitcast.106), channel_id=1, replica_groups=mesh['sp'=8,'tp'=4] {'sp'}, dimensions={1} | all-to-all | bytes 1966080 | tf_op jit(solution)/shard_map/all_to_all | solution.py:148
  134.5 1.5 copy.53
  136.3 31.9 %all-gather.3.cloned.1.call-done = bf16[4,8,30,2048]{3,1,2,0:T(8,128)(2,1)} async-done(((bf16[1,8,30,2048]{3,1,2,0:T(8,128)(2,1)}), bf16[4,8,30,2048]{3,1,2,0:T(8,128)(2,1)}) %all-gather.3.cloned.1.call-update) | async-done | bytes 3932176 | tf_op jit(solution)/shard_map/all_gather | solution.py:150
  168.2 6.3 %copy.54 = bf16[4,8,30,2048]{3,2,1,0:T(8,128)(2,1)} copy(bf16[4,8,30,2048]{3,1,2,0:T(8,128)(2,1)} %all-gather.3.cloned.1.call-done) | data formatting | bytes 7864320 | tf_op jit(solution)/shard_map/all_gather | solution.py:150
  174.5 5.1 %reshape.224 = bf16[960,2048]{1,0:T(8,128)(2,1)} reshape(bf16[4,8,30,2048]{3,2,1,0:T(8,128)(2,1)} %copy.54) | data formatting | bytes 7864320 | tf_op jit(solution)/shard_map/reshape | solution.py:150
  179.6 4.4 %convolution_minimum_fusion = f32[960,256]{1,0:T(8,128)} fusion(bf16[960,2048]{1,0:T(8,128)(2,1)} %reshape.224, bf16[1,2048,256]{2,1,0:T(8,128)(2,1)S(1)} %copy-done.12), kind=kOutput, calls=%fused_computation.34 | convolution fusion | flops 1006878720 | bytes 5963776 | tf_op jit(solution)/shard_map/dot_general | solution.py:45
  184.0 8.7 %convolution_convert_fusion.2 = bf16[960,2048]{1,0:T(8,128)(2,1)} fusion(bf16[960,2048]{1,0:T(8,128)(2,1)} %reshape.224, bf16[1,256,2048]{2,1,0:T(8,128)(2,1)S(1)} %copy-done, bf16[1,2048,256]{2,1,0:T(8,128)(2,1)} %param.30, f32[960,256]{1,0:T(8,128)} %convolution_minimum_fusion), kind=kOutput, calls=%fused_computation.28 | convolution fusion | flops 2017443840 | bytes 10944512 | tf_op jit(solution)/shard_map/dot_general | solution.py:48
  192.7 43.0 %reduce-scatter.2.cloned.1.call-done = bf16[240,2048]{1,0:T(8,128)(2,1)} async-done(((bf16[960,2048]{1,0:T(8,128)(2,1)}), bf16[240,2048]{1,0:T(8,128)(2,1)}) %reduce-scatter.2.cloned.1.call-update) | async-done | bytes 983056 | tf_op jit(solution)/shard_map/reduce_scatter | solution.py:155
  235.8 2.5 reshape.225
  238.2 5.5 %all-to-all-start.1 = ((bf16[1,8,30,2048]{3,2,0,1:T(8,128)(2,1)}), bf16[1,8,30,2048]{3,2,0,1:T(8,128)(2,1)}, u32[]{:S(2)}, u32[]{:S(2)}) async-start(bf16[1,8,30,2048]{3,2,0,1:T(8,128)(2,1)} %bitcast.19), calls=%async_computation.2 | async-start | bytes 2097152 | tf_op jit(solution)/shard_map/all_to_all | solution.py:156
  243.9 25.6 %all-to-all-done.1 = bf16[1,8,30,2048]{3,2,0,1:T(8,128)(2,1)} async-done(((bf16[1,8,30,2048]{3,2,0,1:T(8,128)(2,1)}), bf16[1,8,30,2048]{3,2,0,1:T(8,128)(2,1)}, u32[]{:S(2)}, u32[]{:S(2)}) %all-to-all-start.1) | async-done | bytes 983072 | tf_op jit(solution)/shard_map/all_to_all | solution.py:156
  269.5 1.5 reshape.226
  271.0 2.0 gather_fusion.1
  273.0 2.1 reshape.232
  275.2 2.3 multiply_reduce_fusion
  (121 shorter events, 17.5 us)
Async XLA Ops:
  6.5 177.4 %copy-start = (bf16[1,256,2048]{2,1,0:T(8,128)(2,1)S(1)}, bf16[1,256,2048]{2,1,0:T(8,128)(2,1)}, u32[]{:S(2)}) copy-start(bf16[1,256,2048]{2,1,0:T(8,128)(2,1)} %param.31) | copy-start | bytes 3145732
  6.5 35.9 %copy-start.7 = (bf16[1,96,1024]{2,1,0:T(8,128)(2,1)S(1)}, bf16[1,96,1024]{2,1,0:T(8,128)(2,1)}, u32[]{:S(2)}) copy-start(bf16[1,96,1024]{2,1,0:T(8,128)(2,1)} %param.18) | copy-start | bytes 589828
  6.5 36.0 %copy-start.8 = (bf16[1,96,128]{2,1,0:T(8,128)(2,1)S(1)}, bf16[1,96,128]{2,1,0:T(8,128)(2,1)}, u32[]{:S(2)}) copy-start(bf16[1,96,128]{2,1,0:T(8,128)(2,1)} %param.20) | copy-start | bytes 73732
  6.5 36.2 %copy-start.11 = (f32[128]{0:T(128)S(1)}, f32[128]{0:T(128)}, u32[]{:S(2)}) copy-start(f32[128]{0:T(128)} %param.22) | copy-start | bytes 1540
  6.5 161.7 %all-gather.3.cloned.1.call-start = ((), (), s32[]{:S(2)}) async-start(), calls=%async_computation.3 | async-start | bytes 4915200 | tf_op jit(solution)/shard_map/all_gather | solution.py:150
  75.5 2.0 copy-start.3
  75.6 2.5 copy-start.1
  82.7 0.7 copy-start.2
  82.7 0.7 copy-start.5
  82.7 1.3 copy-start.4
  83.4 0.6 copy-start.6
  84.0 1.9 copy-start.3
  84.0 2.5 copy-start.1
  91.4 0.7 copy-start.2
  91.4 0.7 copy-start.5
  91.4 1.3 copy-start.4
  92.1 0.6 copy-start.6
  92.7 1.9 copy-start.3
  92.7 2.5 copy-start.1
  100.0 0.7 copy-start.2
  100.0 0.7 copy-start.5
  100.0 1.3 copy-start.4
  100.7 0.6 copy-start.6
  102.4 6.8 %copy-start.9 = (f32[2048]{0:T(1024)S(1)}, f32[2048]{0:T(1024)}, u32[]{:S(2)}) copy-start(f32[2048]{0:T(1024)} %param.26) | copy-start | bytes 24580
  136.1 99.7 %reduce-scatter.2.cloned.1.call-start = ((), (), s32[]{:S(2)}) async-start(), calls=%async_computation.4 | async-start | bytes 4915200 | tf_op jit(solution)/shard_map/reduce_scatter | solution.py:155
  174.5 5.1 %copy-start.12 = (bf16[1,2048,256]{2,1,0:T(8,128)(2,1)S(1)}, bf16[1,2048,256]{2,1,0:T(8,128)(2,1)}, u32[]{:S(2)}) copy-start(bf16[1,2048,256]{2,1,0:T(8,128)(2,1)} %param.29) | copy-start | bytes 3145732
  192.7 51.0 %copy-start.10 = (f32[1,96,2]{1,2,0:T(2,128)S(1)}, f32[1,96,2]{1,2,0:T(2,128)}, u32[]{:S(2)}) copy-start(f32[1,96,2]{1,2,0:T(2,128)} %param.28) | copy-start | bytes 2308
  238.2 31.3 %all-to-all-start.1 = ((bf16[1,8,30,2048]{3,2,0,1:T(8,128)(2,1)}), bf16[1,8,30,2048]{3,2,0,1:T(8,128)(2,1)}, u32[]{:S(2)}, u32[]{:S(2)}) async-start(bf16[1,8,30,2048]{3,2,0,1:T(8,128)(2,1)} %bitcast.19), calls=%async_computation.2 | async-start | bytes 2097152 | tf_op jit(solution)/shard_map/all_to_all | solution.py:156
Sparse Core Ops, SparseCore 0:
  136.2 31.9 all-gather.2
  192.8 42.8 reduce-scatter.1
where the time goes:
time: 286 us; the launch traced here: 285 us
  waiting for transfers between devices  101 us (35%)
  blocking collectives  86.8 us (30%)
  local copies, waits for them, and re-layouts  34.3 us (12%)
  matrix products  34.2 us (12%)
  between operations  13.7 us (5%)
  other arithmetic  9.43 us (3%)
  starting transfers between devices  5.77 us (2%)
    reduce_scatter x1, waiting for transfers between devices, local(): lax.psum_scatter(terms.astype(jnp.bfloat16), 'tp', scatter_dimension=0, t...  43 us
    all_gather x1, blocking collectives, local(): lax.all_gather(key_turned, 'sp', axis=0, tiled=True)  32.8 us
    all_gather x1, blocking collectives, local(): lax.all_gather(normed, 'sp', axis=0, tiled=True)  32.6 us
    all_gather x1, waiting for transfers between devices, local(): lax.all_gather(arrived, 'tp', axis=0, tiled=True).reshape(-1, width)  31.9 us
    all_to_all x1, waiting for transfers between devices, local(): lax.all_to_all(mine.reshape(1, experts, slots, width), 'sp', split_axis=1...  25.6 us
    all_to_all x1, blocking collectives, local(): lax.all_to_all(outgoing, 'sp', split_axis=1, concat_axis=1, tiled=True)  21.4 us
    dot_general x1, matrix products, expert_term(): return jnp.dot(active, down_w, preferred_element_type=jnp.float32)  8.72 us
    dot_general x3, matrix products, step(): jnp.einsum('hqk,khd->qhd', weights.astype(jnp.bfloat16), values, preferre...  7.3 us
  transfers between devices with their start and end apart: 3, of which 3 were waited for; matrix products, arithmetic and copies ran while one was open for 0% of the time, Pallas kernels for 0%

commit v1 on v0

v1 whole, which is shorter than its diff:
```python
import functools

import jax
import jax.numpy as jnp
from jax import lax
from jax.experimental import pallas as pl
from jax.experimental.pallas import tpu as pltpu
from jax.sharding import PartitionSpec as P

HEADS = 16
NOPE = 64
ROPE = 32
VDIM = 64
LATENT = 128
TOPK = 2
LANES = 128

EPS = 1e-06
ROPE_BASE = 10000.0
CLAMP = 7.0
ALPHA = 1.702
MESH = pl.DeviceIdType.MESH
VM = pl.BlockSpec(memory_space=pltpu.VMEM)
F32 = jnp.float32
BF16 = jnp.bfloat16


def swapped(x):
    lane = lax.broadcasted_iota(jnp.int32, x.shape, 1)
    half = ROPE // 2
    return jnp.where(
        lane % ROPE < half, pltpu.roll(x, x.shape[1] - half, 1), pltpu.roll(x, half, 1)
    )


def prep_kernel(lat_ref, gain_ref, rk_ref, cos_ref, sin_ref, blk_ref):
    lat = lat_ref[...].astype(F32)
    mean = jnp.mean(lat * lat, axis=-1, keepdims=True)
    blk_ref[:, :LATENT] = (lat * lax.rsqrt(mean + EPS) * gain_ref[...]).astype(BF16)
    rk = rk_ref[...].astype(F32)
    blk_ref[:, LATENT:] = (rk * cos_ref[...] + swapped(rk) * sin_ref[...]).astype(BF16)


def place(picks_ref, experts, slots, tokens):
    expert = lax.broadcasted_iota(jnp.int32, (experts, tokens), 0)
    hots = [(expert == picks_ref[k : k + 1, :]).astype(F32) for k in range(TOPK)]
    earlier = (
        lax.broadcasted_iota(jnp.int32, (tokens, tokens), 0)
        < lax.broadcasted_iota(jnp.int32, (tokens, tokens), 1)
    ).astype(F32)
    rank = jnp.dot(sum(hots), earlier, preferred_element_type=F32)
    where = rank + (expert * slots).astype(F32)
    slot = lax.broadcasted_iota(jnp.int32, (experts * slots, tokens), 0).astype(F32)
    return [
        (slot == jnp.sum(hot * where, axis=0, keepdims=True)).astype(F32) for hot in hots
    ]


def attend_kernel(
    n, slots,
    blk_ref, qn_ref, qr_ref, cos_ref, sin_ref, upk_ref, upv_ref, ow_ref, res_ref, gain_ref,
    picks_ref, mid_ref, out_ref, rows, qrot, att, norm, send_sem, recv_sem,
):
    tokens = blk_ref.shape[0]
    width = res_ref.shape[1]
    me = lax.axis_index("sp")
    barrier = pltpu.get_barrier_semaphore()
    for d in range(1, n):
        pl.semaphore_signal(
            barrier, inc=1, device_id={"sp": lax.rem(me + d, n)}, device_id_type=MESH
        )
    pl.semaphore_wait(barrier, n - 1)
    copies = []
    for d in range(1, n):
        copy = pltpu.make_async_remote_copy(
            src_ref=blk_ref,
            dst_ref=rows.at[pl.ds(d * tokens, tokens)],
            send_sem=send_sem.at[d],
            recv_sem=recv_sem.at[d],
            device_id={"sp": lax.rem(me + d, n)},
            device_id_type=MESH,
        )
        copy.start()
        copies.append(copy)
    rows[:tokens, :] = blk_ref[...]
    for g in range(HEADS * ROPE // LANES):
        x = qr_ref[:, g * LANES : (g + 1) * LANES].astype(F32)
        qrot[:, g * LANES : (g + 1) * LANES] = (
            x * cos_ref[...] + swapped(x) * sin_ref[...]
        ).astype(BF16)
    factor = (NOPE + ROPE) ** (-0.5)
    lane = lax.broadcasted_iota(jnp.int32, (tokens, LANES), 1)
    low = lane < NOPE
    lowb = low.astype(F32).astype(BF16)
    highb = (lane >= NOPE).astype(F32).astype(BF16)
    ropeb = [(lane // ROPE == k).astype(F32).astype(BF16) for k in range(LANES // ROPE)]
    for copy in copies:
        copy.wait()

    def group(g, carry):
        turned = qrot[:, pl.ds(pl.multiple_of(g * LANES, LANES), LANES)]
        for q in range(2):
            lanes = pl.ds(pl.multiple_of((g * 2 + q) * LANES, LANES), LANES)
            lat = rows[:, :LATENT]
            keys = jnp.dot(lat, upk_ref[:, lanes], preferred_element_type=F32).astype(BF16)
            vals = jnp.dot(lat, upv_ref[:, lanes], preferred_element_type=F32).astype(BF16)
            keys = jnp.concatenate([keys, rows[:, LATENT:]], axis=1)
            plain = qn_ref[:, lanes]
            first = jnp.concatenate([plain * lowb, turned * ropeb[2 * q]], axis=1)
            second = jnp.concatenate([plain * highb, turned * ropeb[2 * q + 1]], axis=1)
            query = jnp.concatenate([first, second], axis=0)
            scores = lax.dot_general(
                query, keys, (((1,), (1,)), ((), ())), preferred_element_type=F32
            ) * factor
            weights = jnp.exp(scores - jnp.max(scores, axis=-1, keepdims=True))
            total = jnp.sum(weights, axis=-1, keepdims=True)
            mixed = jnp.dot(weights.astype(BF16), vals, preferred_element_type=F32) / total
            att[:, lanes] = jnp.where(low, mixed[:tokens], mixed[tokens:]).astype(BF16)
        return carry

    lax.fori_loop(0, HEADS * ROPE // LANES, group, 0)
    step = 512

    def project(c, square):
        cols = pl.ds(pl.multiple_of(c * step, step), step)
        product = jnp.dot(att[...], ow_ref[:, cols], preferred_element_type=F32)
        middle = (res_ref[:, cols].astype(F32) + product).astype(BF16)
        mid_ref[:, cols] = middle
        wide = middle.astype(F32)
        return square + jnp.sum(wide * wide, axis=-1, keepdims=True)

    square = lax.fori_loop(0, width // step, project, jnp.zeros((tokens, 1), F32))
    scale = lax.rsqrt(square / width + EPS)
    norm[...] = (mid_ref[...].astype(F32) * scale * gain_ref[...]).astype(BF16)
    packer = sum(place(picks_ref, n, slots, tokens)).astype(BF16)

    def pack(c, carry):
        cols = pl.ds(pl.multiple_of(c * step, step), step)
        out_ref[:, cols] = jnp.dot(packer, norm[:, cols], preferred_element_type=F32).astype(BF16)
        return carry

    lax.fori_loop(0, width // step, pack, 0)


def combine_kernel(n, slots, mid_ref, back_ref, picks_ref, weight_ref, out_ref):
    tokens, width = mid_ref.shape
    spots = place(picks_ref, n, slots, tokens)
    high = low = 0.0
    for k in range(TOPK):
        weight = weight_ref[k : k + 1, :]
        coarse = weight.astype(BF16).astype(F32)
        high = high + spots[k] * coarse
        low = low + spots[k] * (weight - coarse)
    high = high.astype(BF16)
    low = low.astype(BF16)
    dims = (((0,), (0,)), ((), ()))
    step = 512

    def chunk(c, carry):
        cols = pl.ds(pl.multiple_of(c * step, step), step)
        back = back_ref[:, cols]
        added = lax.dot_general(high, back, dims, preferred_element_type=F32)
        added = added + lax.dot_general(low, back, dims, preferred_element_type=F32)
        out_ref[:, cols] = (mid_ref[:, cols].astype(F32) + added).astype(BF16)
        return carry

    lax.fori_loop(0, width // step, chunk, 0)


def expert_term(rows, gate_w, up_w, down_w):
    gate = jnp.minimum(jnp.dot(rows, gate_w, preferred_element_type=F32), CLAMP)
    lift = jnp.clip(jnp.dot(rows, up_w, preferred_element_type=F32), -CLAMP, CLAMP)
    active = (gate * jax.nn.sigmoid(ALPHA * gate) * (lift + 1.0)).astype(BF16)
    return jnp.dot(active, down_w, preferred_element_type=F32)


def local(
    residual, query_nope, query_rope, latent, rope_key, latent_gain, up_key, up_value,
    out_weight, ffn_gain, routes, route_weight, gate_weight, up_weight, down_weight,
):
    tokens, width = residual.shape[1:]
    n = lax.axis_size("sp")
    slots = min(tokens, max(2, 5 * tokens * TOPK // (4 * n)))
    slots = -(-slots // 16) * 16
    positions = lax.axis_index("sp") * tokens + jnp.arange(tokens, dtype=jnp.int32)
    lane = jnp.arange(LANES, dtype=jnp.int32)
    half = ROPE // 2
    inverse = ROPE_BASE ** (-(lane % half).astype(F32) * 2.0 / ROPE)
    angle = positions.astype(F32)[:, None] * inverse[None, :]
    cosine = jnp.cos(angle)
    sine = jnp.sin(angle) * jnp.where(lane % ROPE < half, -1.0, 1.0)[None, :]
    blk = pl.pallas_call(
        prep_kernel,
        out_shape=jax.ShapeDtypeStruct((tokens, 2 * LANES), BF16),
        in_specs=[VM] * 5,
        out_specs=VM,
    )(latent[0], latent_gain[None, :], jnp.tile(rope_key[0], (1, LANES // ROPE)), cosine, sine)
    picks = lax.dynamic_index_in_dim(
        jnp.transpose(routes, (0, 2, 1)), lax.axis_index("tp"), 0, keepdims=False
    )
    middle, outgoing = pl.pallas_call(
        functools.partial(attend_kernel, n, slots),
        out_shape=(
            jax.ShapeDtypeStruct((tokens, width), BF16),
            jax.ShapeDtypeStruct((n * slots, width), BF16),
        ),
        in_specs=[VM] * 11,
        out_specs=(VM, VM),
        scratch_shapes=[
            pltpu.VMEM((n * tokens, 2 * LANES), BF16),
            pltpu.VMEM((tokens, HEADS * ROPE), BF16),
            pltpu.VMEM((tokens, HEADS * VDIM), BF16),
            pltpu.VMEM((tokens, width), BF16),
            pltpu.SemaphoreType.DMA((n,)),
            pltpu.SemaphoreType.DMA((n,)),
        ],
        compiler_params=pltpu.CompilerParams(
            collective_id=0, has_side_effects=True, vmem_limit_bytes=60 * 2**20
        ),
    )(
        blk, query_nope[0], query_rope[0], cosine, sine, up_key, up_value, out_weight,
        residual[0], ffn_gain[None, :], picks,
    )
    arrived = lax.all_to_all(
        outgoing.reshape(1, n, slots, width), "sp", split_axis=1, concat_axis=1, tiled=True
    ).reshape(n * slots, width)
    gathered = lax.all_gather(arrived, "tp", axis=0, tiled=True)
    terms = expert_term(gathered, gate_weight[0], up_weight[0], down_weight[0])
    mine = lax.psum_scatter(terms.astype(BF16), "tp", scatter_dimension=0, tiled=True)
    returned = lax.all_to_all(
        mine.reshape(1, n, slots, width), "sp", split_axis=1, concat_axis=1, tiled=True
    )
    updated = pl.pallas_call(
        functools.partial(combine_kernel, n, slots),
        out_shape=jax.ShapeDtypeStruct((tokens, width), BF16),
        in_specs=[VM] * 4,
        out_specs=VM,
    )(middle, returned.reshape(n * slots, width), picks, jnp.transpose(route_weight[0], (1, 0)))
    return updated[None]


def solution(mesh):
    in_specs = (
        P("tp", "sp", None),
        P("tp", "sp", None),
        P("tp", "sp", None),
        P("tp", "sp", None),
        P("tp", "sp", None),
        P(),
        P(),
        P(),
        P(),
        P(),
        P(None, "sp", None),
        P("tp", "sp", None),
        P("sp", None, "tp"),
        P("sp", None, "tp"),
        P("sp", "tp", None),
    )
    out_specs = P("tp", "sp", None)
    return jax.shard_map(local, mesh=mesh, in_specs=in_specs, out_specs=out_specs, check_vma=False)
```

time: 286 us -> 202 us (0.71)
  local copies, waits for them, and re-layouts: 34.3 us -> 2.77 us
  Pallas kernels: 0 us -> 29.4 us
  blocking collectives: 86.8 us -> 63.8 us
  waiting for transfers between devices: 101 us -> 78.3 us
  matrix products: 34.2 us -> 13.4 us
  other arithmetic: 9.43 us -> 0.91 us
  starting transfers between devices: 5.77 us -> 0.04 us
    all_gather x2 -> x0, blocking collectives: 65.4 us -> none  [the longest x1 32.8 us: local(): lax.all_gather(key_turned, 'sp', axis=0, tiled=True)]
    all_to_all x1 -> x2, blocking collectives: 21.4 us -> 63.8 us  [the longest x1 32.6 us: local(): lax.all_to_all(outgoing.reshape(1, n, slots, width), 'sp', split_axis=1,...]
    pallas_call x0 -> x3, Pallas kernels: none -> 29.4 us  [the longest x1 24.6 us: local(): pl.pallas_call(functools.partial(attend_kernel, n, slots), out_shape=(jax...]
    all_to_all x1 -> x0, waiting for transfers between devices: 25.6 us -> none  [local(): lax.all_to_all(mine.reshape(1, experts, slots, width), 'sp', split_axis=1...]
    dot_general x18 -> x2, matrix products: 34.2 us -> 13.4 us  [the longest x1 8.86 us: expert_term(): return jnp.dot(active, down_w, preferred_element_type=F32)]
    reshape x5 -> x0, local copies, waits for them, and re-layouts: 10.5 us -> none  [the longest x1 5.1 us: local(): lax.all_gather(arrived, 'tp', axis=0, tiled=True).reshape(-1, width)]
    convert_element_type x8 -> x0, local copies, waits for them, and re-layouts: 6.76 us -> none  [the longest x3 3.02 us: step(): jnp.dot(blocks[0], up_value, preferred_element_type=jnp.float32)]
    all_gather x2 -> x0, local copies, waits for them, and re-layouts: 6.57 us -> none  [the longest x1 6.31 us: local(): lax.all_gather(arrived, 'tp', axis=0, tiled=True).reshape(-1, width)]
  transfers between devices with their start and end apart: 3 -> 2, of which waited for: 3 -> 2; matrix products, arithmetic and copies ran while one was open for 0% -> 0% of each run, Pallas kernels for 0% -> 0%
where the time goes in v1:
time: 202 us
  waiting for transfers between devices  78.3 us (39%)
  blocking collectives  63.8 us (32%)
  Pallas kernels  29.4 us (15%)
  matrix products  13.4 us (7%)
  between operations  13.4 us (7%)
  local copies, waits for them, and re-layouts  2.77 us (1%)
    reduce_scatter x1, waiting for transfers between devices, local(): lax.psum_scatter(terms.astype(BF16), 'tp', scatter_dimension=0, tiled=True)  44.7 us
    all_gather x1, waiting for transfers between devices, local(): gathered = lax.all_gather(arrived, 'tp', axis=0, tiled=True)  33.5 us
    all_to_all x1, blocking collectives, local(): lax.all_to_all(outgoing.reshape(1, n, slots, width), 'sp', split_axis=1,...  32.6 us
    all_to_all x1, blocking collectives, local(): lax.all_to_all(mine.reshape(1, n, slots, width), 'sp', split_axis=1, conc...  31.2 us
    pallas_call x1, Pallas kernels, local(): pl.pallas_call(functools.partial(attend_kernel, n, slots), out_shape=(jax...  24.6 us
    dot_general x1, matrix products, expert_term(): return jnp.dot(active, down_w, preferred_element_type=F32)  8.86 us
    dot_general x1, matrix products, expert_term(): gate = jnp.minimum(jnp.dot(rows, gate_w, preferred_element_type=F32), CLAMP)  4.5 us
  transfers between devices with their start and end apart: 2, of which 2 were waited for; matrix products, arithmetic and copies ran while one was open for 0% of the time, Pallas kernels for 0%

profile of v1, /device:TPU:0, one launch (start us, length us, event | category | flops | bytes accessed | tf_op | source)
XLA Modules:
  0.0 202.0 jit_solution(560257799544146039)
XLA Ops:
  6.5 0.0 copy-start
  6.5 0.0 all-gather.2.cloned.1.call-start
  6.6 0.8 tile.11
  7.4 0.7 copy.18.rk_ref
  8.1 1.3 dynamic-slice_bitcast_fusion.picks_ref
  9.3 0.9 fusion.17
  10.2 1.6 shard_map.145.blk_ref
  11.8 0.0 copy-start.1
  11.8 24.6 %shard_map.146 = (bf16[96,2048]{1,0:T(8,128)(2,1)}, bf16[256,2048]{1,0:T(8,128)(2,1)}) custom-call(bf16[96,256]{1,0:T(8,128)(2,1)} %shard_map.145.blk_ref, bf16[96,1024]{1,0:T(8,128)(2,1)} %bitcast.41, bf16[96,512]{1,0:T(8,128)(2,1)} %bitcast.43, f32[96,128]{1,0:T(8,128)} %get-tuple-element.10.cos_ref, f32[96,128]{1,0:T(8,128)} %get-tuple-element.9.sin_ref, ...), custom_call_target="tpu_custom_call" | custom-call | tf_op jit(solution)/shard_map/pallas_call | solution.py:201
  36.4 32.6 %all_to_all.10 = bf16[1,8,32,2048]{3,2,0,1:T(8,128)(2,1)} all-to-all(bf16[1,8,32,2048]{3,2,0,1:T(8,128)(2,1)} %bitcast.39), channel_id=1, replica_groups=mesh['sp'=8,'tp'=4] {'sp'}, dimensions={1} | all-to-all | bytes 2097152 | tf_op jit(solution)/shard_map/all_to_all | solution.py:224
  69.0 0.0 copy-start.2
  69.0 0.0 all-gather.2.cloned.1.call-update
  69.0 0.0 reduce-scatter.2.cloned.1.call-start
  69.1 33.5 %all-gather.2.cloned.1.call-done = bf16[1024,2048]{1,0:T(8,128)(2,1)} async-done(((bf16[256,2048]{1,0:T(8,128)(2,1)}), bf16[1024,2048]{1,0:T(8,128)(2,1)}) %all-gather.2.cloned.1.call-update) | async-done | bytes 4194320 | tf_op jit(solution)/shard_map/all_gather | solution.py:227
  102.6 0.0 copy-done.1
  102.6 4.5 %convolution_minimum_fusion = f32[1024,256]{1,0:T(8,128)} fusion(bf16[1024,2048]{1,0:T(8,128)(2,1)} %all-gather.2.cloned.1.call-done, bf16[1,2048,256]{2,1,0:T(8,128)(2,1)S(1)} %copy-done.1), kind=kOutput, calls=%fused_computation.1 | convolution fusion | flops 1074003968 | bytes 6291456 | tf_op jit(solution)/shard_map/dot_general | solution.py:171
  107.1 0.0 copy-done
  107.1 0.0 copy-done.2
  107.1 8.9 %convolution_convert_fusion = bf16[1024,2048]{1,0:T(8,128)(2,1)} fusion(bf16[1024,2048]{1,0:T(8,128)(2,1)} %all-gather.2.cloned.1.call-done, bf16[1,256,2048]{2,1,0:T(8,128)(2,1)S(1)} %copy-done, bf16[1,2048,256]{2,1,0:T(8,128)(2,1)S(1)} %copy-done.2, f32[1024,256]{1,0:T(8,128)} %convolution_minimum_fusion), kind=kOutput, calls=%fused_computation | convolution fusion | flops 2151940096 | bytes 11534336 | tf_op jit(solution)/shard_map/dot_general | solution.py:174
  115.9 0.0 reduce-scatter.2.cloned.1.call-update
  116.0 44.7 %reduce-scatter.2.cloned.1.call-done = bf16[256,2048]{1,0:T(8,128)(2,1)} async-done(((bf16[1024,2048]{1,0:T(8,128)(2,1)}), bf16[256,2048]{1,0:T(8,128)(2,1)}) %reduce-scatter.2.cloned.1.call-update) | async-done | bytes 1048592 | tf_op jit(solution)/shard_map/reduce_scatter | solution.py:229
  160.7 31.2 %all_to_all.11 = bf16[1,8,32,2048]{3,2,0,1:T(8,128)(2,1)} all-to-all(bf16[1,8,32,2048]{3,2,0,1:T(8,128)(2,1)} %bitcast.38), channel_id=1, replica_groups=mesh['sp'=8,'tp'=4] {'sp'}, dimensions={1} | all-to-all | bytes 2097152 | tf_op jit(solution)/shard_map/all_to_all | solution.py:230
  191.9 3.3 %shard_map.147 = bf16[96,2048]{1,0:T(8,128)(2,1)} custom-call(bf16[96,2048]{1,0:T(8,128)(2,1)} %get-tuple-element.7.mid_ref, bf16[256,2048]{1,0:T(8,128)(2,1)} %bitcast.37, s32[2,96]{1,0:T(2,128)} %dynamic-slice_bitcast_fusion.picks_ref, f32[2,96]{1,0:T(2,128)} %bitcast.47), custom_call_target="tpu_custom_call" | custom-call | tf_op jit(solution)/shard_map/pallas_call | solution.py:233
  (2 shorter events, 0.0 us)
Async XLA Ops:
  6.5 100.6 %copy-start = (bf16[1,256,2048]{2,1,0:T(8,128)(2,1)S(1)}, bf16[1,256,2048]{2,1,0:T(8,128)(2,1)}, u32[]{:S(2)}) copy-start(bf16[1,256,2048]{2,1,0:T(8,128)(2,1)} %param.29) | copy-start | bytes 3145732
  6.5 96.0 %all-gather.2.cloned.1.call-start = ((), (), s32[]{:S(2)}) async-start(), calls=%async_computation.3 | async-start | bytes 5242880 | tf_op jit(solution)/shard_map/all_gather | solution.py:227
  11.8 90.8 %copy-start.1 = (bf16[1,2048,256]{2,1,0:T(8,128)(2,1)S(1)}, bf16[1,2048,256]{2,1,0:T(8,128)(2,1)}, u32[]{:S(2)}) copy-start(bf16[1,2048,256]{2,1,0:T(8,128)(2,1)} %param.27) | copy-start | bytes 3145732
  69.0 38.1 %copy-start.2 = (bf16[1,2048,256]{2,1,0:T(8,128)(2,1)S(1)}, bf16[1,2048,256]{2,1,0:T(8,128)(2,1)}, u32[]{:S(2)}) copy-start(bf16[1,2048,256]{2,1,0:T(8,128)(2,1)} %param.28) | copy-start | bytes 3145732
  69.0 91.7 %reduce-scatter.2.cloned.1.call-start = ((), (), s32[]{:S(2)}) async-start(), calls=%async_computation.4 | async-start | bytes 5242880 | tf_op jit(solution)/shard_map/reduce_scatter | solution.py:229
Sparse Core Ops, SparseCore 0:
  69.1 33.4 all-gather.1
  116.1 44.5 reduce-scatter.1

commit v2 on v1

--- a/solution.py
+++ b/solution.py
@@ -142,8 +142,134 @@
     lax.fori_loop(0, width // step, pack, 0)
 
 
-def combine_kernel(n, slots, mid_ref, back_ref, picks_ref, weight_ref, out_ref):
+def expert_kernel(
+    n, m, slots,
+    sent_ref, gate_ref, up_ref, down_ref, mid_ref, picks_ref, weight_ref, out_ref,
+    held, red, fin, back, local_sem, send_sem, recv_sem,
+):
     tokens, width = mid_ref.shape
+    groups = m // 2
+    me = lax.axis_index("sp")
+    rank = lax.axis_index("tp")
+    sibling = rank + 1 - 2 * lax.rem(rank, 2)
+    parts = min(4, n)
+    count = n // parts
+    span = count * slots
+    step = 512
+    barrier = pltpu.get_barrier_semaphore()
+    for d in range(1, n):
+        pl.semaphore_signal(
+            barrier, inc=1, device_id={"sp": lax.rem(me + d, n)}, device_id_type=MESH
+        )
+    for j in range(1, groups):
+        pl.semaphore_signal(
+            barrier, inc=1, device_id={"tp": lax.rem(rank + 2 * j, m)}, device_id_type=MESH
+        )
+    pl.semaphore_signal(barrier, inc=1, device_id={"tp": sibling}, device_id_type=MESH)
+    pl.semaphore_wait(barrier, n + groups - 1)
+    used = [0]
+
+    def remote(source, target, device):
+        index = used[0]
+        used[0] += 1
+        copy = pltpu.make_async_remote_copy(
+            src_ref=source,
+            dst_ref=target,
+            send_sem=send_sem.at[index],
+            recv_sem=recv_sem.at[index],
+            device_id=device,
+            device_id_type=MESH,
+        )
+        copy.start()
+        return copy
+
+    first = pltpu.make_async_copy(
+        sent_ref.at[pl.ds(me * slots, slots)], held.at[0, 0, pl.ds(0, slots)], local_sem
+    )
+    first.start()
+    arrive = [first]
+    for d in range(1, n):
+        peer = lax.rem(me + d, n)
+        arrive.append(
+            remote(
+                sent_ref.at[pl.ds(peer * slots, slots)],
+                held.at[0, 0, pl.ds(d * slots, slots)],
+                {"sp": peer},
+            )
+        )
+    across, aside, reduced, final, returned = {}, {}, {}, {}, {}
+
+    def forward(k):
+        rows = pl.ds(k * span, span)
+        for d in range(k * count, (k + 1) * count):
+            arrive[d].wait()
+        for j in range(1, groups):
+            across[k, j] = remote(
+                held.at[0, 0, rows], held.at[j, 0, rows], {"tp": lax.rem(rank + 2 * j, m)}
+            )
+        aside[k, 0] = remote(held.at[0, 0, rows], held.at[0, 1, rows], {"tp": sibling})
+
+    def relay(k):
+        rows = pl.ds(k * span, span)
+        for j in range(1, groups):
+            across[k, j].wait()
+            aside[k, j] = remote(held.at[j, 0, rows], held.at[j, 1, rows], {"tp": sibling})
+
+    def compute(k):
+        rows = pl.ds(k * span, span)
+        for j in range(groups):
+            aside[k, j].wait()
+        block = jnp.concatenate(
+            [held[j, c, rows, :] for j in range(groups) for c in range(2)], axis=0
+        )
+        gate = jnp.minimum(jnp.dot(block, gate_ref[...], preferred_element_type=F32), CLAMP)
+        lift = jnp.clip(
+            jnp.dot(block, up_ref[...], preferred_element_type=F32), -CLAMP, CLAMP
+        )
+        active = (gate * jax.nn.sigmoid(ALPHA * gate) * (lift + 1.0)).astype(BF16)
+
+        def down(c, carry):
+            cols = pl.ds(pl.multiple_of(c * step, step), step)
+            term = jnp.dot(active, down_ref[:, cols], preferred_element_type=F32).astype(BF16)
+            for i in range(m):
+                held[i // 2, i % 2, rows, cols] = term[i * span : (i + 1) * span]
+            return carry
+
+        lax.fori_loop(0, width // step, down, 0)
+        for j in range(groups):
+            reduced[k, j] = remote(held.at[j, 1, rows], red.at[j, rows], {"tp": sibling})
+
+    def reduce(k):
+        rows = pl.ds(k * span, span)
+        for j in list(range(1, groups)) + [0]:
+            reduced[k, j].wait()
+            total = held[j, 0, rows, :].astype(F32) + red[j, rows, :].astype(F32)
+            held[j, 0, rows, :] = total.astype(BF16)
+            if j:
+                final[k, j] = remote(
+                    held.at[j, 0, rows], fin.at[j - 1, rows], {"tp": lax.rem(rank + m - 2 * j, m)}
+                )
+
+    def finish(k):
+        rows = pl.ds(k * span, span)
+        total = held[0, 0, rows, :].astype(F32)
+        for j in range(1, groups):
+            final[k, j].wait()
+            total = total + fin[j - 1, rows, :].astype(F32)
+        held[0, 0, rows, :] = total.astype(BF16)
+        for d in range(k * count, (k + 1) * count):
+            source = held.at[0, 0, pl.ds(d * slots, slots)]
+            target = back.at[pl.ds(me * slots, slots)]
+            if d:
+                returned[d] = remote(source, target, {"sp": lax.rem(me + n - d, n)})
+            else:
+                returned[d] = pltpu.make_async_copy(source, target, local_sem)
+                returned[d].start()
+
+    for t in range(parts + 4):
+        for work, k in ((forward, t), (relay, t - 1), (compute, t - 2), (reduce, t - 3), (finish, t - 4)):
+            if 0 <= k < parts:
+                work(k)
     spots = place(picks_ref, n, slots, tokens)
     high = low = 0.0
     for k in range(TOPK):
@@ -154,24 +280,18 @@
     high = high.astype(BF16)
     low = low.astype(BF16)
     dims = (((0,), (0,)), ((), ()))
-    step = 512
+    for d in range(n):
+        returned[d].wait()
 
     def chunk(c, carry):
         cols = pl.ds(pl.multiple_of(c * step, step), step)
-        back = back_ref[:, cols]
-        added = lax.dot_general(high, back, dims, preferred_element_type=F32)
-        added = added + lax.dot_general(low, back, dims, preferred_element_type=F32)
+        rows = back[:, cols]
+        added = lax.dot_general(high, rows, dims, preferred_element_type=F32)
+        added = added + lax.dot_general(low, rows, dims, preferred_element_type=F32)
         out_ref[:, cols] = (mid_ref[:, cols].astype(F32) + added).astype(BF16)
         return carry
 
     lax.fori_loop(0, width // step, chunk, 0)
-
-
-def expert_term(rows, gate_w, up_w, down_w):
-    gate = jnp.minimum(jnp.dot(rows, gate_w, preferred_element_type=F32), CLAMP)
-    lift = jnp.clip(jnp.dot(rows, up_w, preferred_element_type=F32), -CLAMP, CLAMP)
-    active = (gate * jax.nn.sigmoid(ALPHA * gate) * (lift + 1.0)).astype(BF16)
-    return jnp.dot(active, down_w, preferred_element_type=F32)
 
 
 def local(
@@ -221,21 +341,29 @@
         blk, query_nope[0], query_rope[0], cosine, sine, up_key, up_value, out_weight,
         residual[0], ffn_gain[None, :], picks,
     )
-    arrived = lax.all_to_all(
-        outgoing.reshape(1, n, slots, width), "sp", split_axis=1, concat_axis=1, tiled=True
-    ).reshape(n * slots, width)
-    gathered = lax.all_gather(arrived, "tp", axis=0, tiled=True)
-    terms = expert_term(gathered, gate_weight[0], up_weight[0], down_weight[0])
-    mine = lax.psum_scatter(terms.astype(BF16), "tp", scatter_dimension=0, tiled=True)
-    returned = lax.all_to_all(
-        mine.reshape(1, n, slots, width), "sp", split_axis=1, concat_axis=1, tiled=True
-    )
+    m = lax.axis_size("tp")
+    copies = 2 * (n - 1) + min(4, n) * (4 * (m // 2) - 2)
     updated = pl.pallas_call(
-        functools.partial(combine_kernel, n, slots),
+        functools.partial(expert_kernel, n, m, slots),
         out_shape=jax.ShapeDtypeStruct((tokens, width), BF16),
-        in_specs=[VM] * 4,
+        in_specs=[VM] * 7,
         out_specs=VM,
-    )(middle, returned.reshape(n * slots, width), picks, jnp.transpose(route_weight[0], (1, 0)))
+        scratch_shapes=[
+            pltpu.VMEM((m // 2, 2, n * slots, width), BF16),
+            pltpu.VMEM((m // 2, n * slots, width), BF16),
+            pltpu.VMEM((max(1, m // 2 - 1), n * slots, width), BF16),
+            pltpu.VMEM((n * slots, width), BF16),
+            pltpu.SemaphoreType.DMA,
+            pltpu.SemaphoreType.DMA((copies,)),
+            pltpu.SemaphoreType.DMA((copies,)),
+        ],
+        compiler_params=pltpu.CompilerParams(
+            collective_id=1, has_side_effects=True, vmem_limit_bytes=60 * 2**20
+        ),
+    )(
+        outgoing, gate_weight[0], up_weight[0], down_weight[0], middle, picks,
+        jnp.transpose(route_weight[0], (1, 0)),
+    )
     return updated[None]
 
 

time: 202 us -> 113 us (0.56)
  Pallas kernels: 29.4 us -> 108 us
  waiting for transfers between devices: 78.3 us -> 0 us
  blocking collectives: 63.8 us -> 0 us
  matrix products: 13.4 us -> 0 us
  between operations: 13.4 us -> 0.02 us
    pallas_call x1, Pallas kernels: 3.25 us -> 81.5 us  [local(): pl.pallas_call(functools.partial(expert_kernel, n, m, slots), out_shape=j...]
    all_to_all x2 -> x0, blocking collectives: 63.8 us -> none  [the longest x1 32.6 us: local(): lax.all_to_all(outgoing.reshape(1, n, slots, width), 'sp', split_axis=1,...]
    reduce_scatter x1 -> x0, waiting for transfers between devices: 44.7 us -> none  [local(): lax.psum_scatter(terms.astype(BF16), 'tp', scatter_dimension=0, tiled=True)]
    all_gather x1 -> x0, waiting for transfers between devices: 33.5 us -> none  [local(): gathered = lax.all_gather(arrived, 'tp', axis=0, tiled=True)]
    dot_general x2 -> x0, matrix products: 13.4 us -> none  [the longest x1 8.86 us: expert_term(): return jnp.dot(active, down_w, preferred_element_type=F32)]
    unnamed x6 -> x3, local copies, waits for them, and re-layouts: 0.01 us -> 2.45 us
  transfers between devices with their start and end apart: 2 -> 0, of which waited for: 2 -> 0; matrix products, arithmetic and copies ran while one was open for 0% -> 0% of each run, Pallas kernels for 0% -> 0%
where the time goes in v2:
time: 113 us
  Pallas kernels  108 us (96%)
  local copies, waits for them, and re-layouts  4.44 us (4%)
    pallas_call x1, Pallas kernels, local(): pl.pallas_call(functools.partial(expert_kernel, n, m, slots), out_shape=j...  81.5 us
    pallas_call x1, Pallas kernels, local(): pl.pallas_call(functools.partial(attend_kernel, n, slots), out_shape=(jax...  24.5 us
    unnamed x3, local copies, waits for them, and re-layouts  2.45 us

profile of v2, /device:TPU:0, one launch (start us, length us, event | category | flops | bytes accessed | tf_op | source)
XLA Modules:
  0.0 113.0 jit_solution(10924900531564826999)
XLA Ops:
  0.0 0.0 copy-start
  0.0 0.7 copy-done
  0.7 0.6 dynamic-slice_bitcast_fusion.picks_ref
  1.3 0.7 tile.11
  2.0 0.7 copy.17.rk_ref
  2.7 0.9 fusion
  3.6 1.6 %shard_map.145.blk_ref = bf16[96,256]{1,0:T(8,128)(2,1)} custom-call(bf16[96,128]{1,0:T(8,128)(2,1)} %bitcast.27, f32[1,128]{1,0:T(1,128)} %bitcast.31, bf16[96,128]{1,0:T(8,128)(2,1)} %copy.17.rk_ref, f32[96,128]{1,0:T(8,128)} %get-tuple-element.10.cos_ref, f32[96,128]{1,0:T(8,128)} %get-tuple-element.9.sin_ref), custom_call_target="tpu_custom_call" | custom-call | tf_op jit(solution)/shard_map/pallas_call | solution.py:312
  5.2 24.5 %shard_map.146 = (bf16[96,2048]{1,0:T(8,128)(2,1)}, bf16[256,2048]{1,0:T(8,128)(2,1)}) custom-call(bf16[96,256]{1,0:T(8,128)(2,1)} %shard_map.145.blk_ref, bf16[96,1024]{1,0:T(8,128)(2,1)} %bitcast.24, bf16[96,512]{1,0:T(8,128)(2,1)} %bitcast.26, f32[96,128]{1,0:T(8,128)} %get-tuple-element.10.cos_ref, f32[96,128]{1,0:T(8,128)} %get-tuple-element.9.sin_ref, ...), custom_call_target="tpu_custom_call" | custom-call | tf_op jit(solution)/shard_map/pallas_call | solution.py:321
  29.7 81.5 %shard_map.147 = bf16[96,2048]{1,0:T(8,128)(2,1)} custom-call(bf16[256,2048]{1,0:T(8,128)(2,1)} %get-tuple-element.7.sent_ref, bf16[2048,256]{1,0:T(8,128)(2,1)} %bitcast.20, bf16[2048,256]{1,0:T(8,128)(2,1)} %bitcast.21, bf16[256,2048]{1,0:T(8,128)(2,1)} %bitcast.22, bf16[96,2048]{1,0:T(8,128)(2,1)} %get-tuple-element.8.mid_ref, ...), custom_call_target="tpu_custom_call" | custom-call | tf_op jit(solution)/shard_map/pallas_call | solution.py:346
  111.2 1.8 %copy.19 = bf16[1,96,2048]{2,1,0:T(8,128)(2,1)} copy(bf16[1,96,2048]{2,1,0:T(8,128)(2,1)} %bitcast.19) | data formatting | bytes 786432
  (2 shorter events, 0.0 us)
Async XLA Ops:
  0.0 0.7 copy-start
